TPU v7x, 32 devices: a whole 2x2x4 slice. The times are simulated.
32 devices in a mesh: ep: 8 (over z, core), tp: 4 (over y, x).
Axes of the slice: x: 2, y: 2, z: 4, core: 2. Of those that a mesh axis runs over, the one named last changes fastest.
Arguments:
- tokens: bfloat16 [1024, 2048], P('ep', 'tp'), may hold values from -6 to 6
- owner_shard: int32 [32768, 1], P('ep'), may hold values from 0 to 7; in each aligned block of 4096 rows (0 to 4095, 4096 to 8191, ...) at most 1024 rows name the same one
- local_row: int32 [32768, 1], P('ep'), may hold values from 0 to 4095
- gate_weights: float32 [1024, 32], P('ep'), may hold values from 0.05 to 1
- up_table: bfloat16 [32768, 2048], P('ep', 'tp'), may hold values from -0.125 to 0.125
- down_table: bfloat16 [32768, 2048], P('ep', 'tp'), may hold values from -6 to 6
Outputs:
- mixed: bfloat16 [1024, 2048], P('ep', 'tp')
Inputs may be any that keep to these rules, and one draw needn't show every extreme that they name: `owner_shard`: within the rows of one device (128 tokens of 32 slots each, token by token) no shard is named by more than 1024 slots, a bound that some block reaches; every shard is named somewhere.
All inputs are finite; a program needn't handle non-finite values.
Results may differ from a plain program's by a relative error of at most 0.0049.
Values may be sent and summed in bfloat16 or wider, within the bound.
A program may use at most 128 MiB of HBM per device.

v0:
```python
import functools

import jax
import jax.numpy as jnp
from jax import lax
from jax.experimental import pallas as pl
from jax.experimental.pallas import tpu as pltpu
from jax.sharding import PartitionSpec as P

MESH = pl.DeviceIdType.MESH
VMEM_BYTES = 60 * 1024 * 1024


def params(number):
    return pltpu.CompilerParams(
        collective_id=number, has_side_effects=True, vmem_limit_bytes=VMEM_BYTES
    )


def vmem():
    return pl.BlockSpec(memory_space=pltpu.VMEM)


def greet(peers):
    barrier = pltpu.get_barrier_semaphore()
    for peer in peers:
        pl.semaphore_signal(barrier, inc=1, device_id=peer, device_id_type=MESH)
    pl.semaphore_wait(barrier, len(peers))


def remote(src, dst, send_sem, recv_sem, peer):
    return pltpu.make_async_remote_copy(
        src_ref=src, dst_ref=dst, send_sem=send_sem, recv_sem=recv_sem,
        device_id=peer, device_id_type=MESH,
    )


def fused_kernel(n_ep, n_tp, slots, tok_ref, aux_ref, up_hbm, down_hbm, out_ref,
                 all_tok, all_aux, up_buf, down_buf, hi_ref, lo_ref, acc_ref, pbuf, pgot, wt_ref, w_ref,
                 own, xbuf, ybuf, sbuf, rbuf,
                 local_sem, send, recv, fsend, frecv, up_sem, down_sem, psend, precv,
                 xsend, xrecv, rsend, rrecv):
    chips = n_ep // 2
    me = lax.axis_index("ep")
    core = lax.rem(me, 2)
    chip = me // 2
    part = lax.axis_index("tp")
    partner = {"ep": me + 1 - 2 * core}
    experts, width = up_hbm.shape
    chunks, chunk_rows = up_buf.shape[0], up_buf.shape[1]
    tiles = experts // 128
    first = me * experts
    group, lanes = aux_ref.shape[1], aux_ref.shape[2]
    side = lanes // slots
    block = group * side
    per_tile = 128 // slots

    def at(step):
        return lax.rem(chip + step, chips)

    def counterpart(step):
        return {"ep": at(step) * 2 + core}

    def tp_peer(step):
        return {"tp": lax.rem(part + step, n_tp)}

    up_loads = []
    for c in range(chunks):
        load = pltpu.make_async_copy(up_hbm.at[pl.ds(c * chunk_rows, chunk_rows)], up_buf.at[c], up_sem.at[c])
        load.start()
        up_loads.append(load)
    greet([partner] + [counterpart(d) for d in range(1, chips)] + [tp_peer(d) for d in range(1, n_tp)])

    pairs = ((aux_ref, all_aux), (tok_ref, all_tok))
    started = []
    local = []
    for i, (src, dst) in enumerate(pairs):
        own_copy = pltpu.make_async_copy(src, dst.at[me], local_sem.at[i])
        own_copy.start()
        local.append(own_copy)
        copy = remote(src, dst.at[me], fsend.at[i, 0], frecv.at[i, 0], partner)
        copy.start()
        started.append(copy)
    for d in range(1, chips):
        for i, (src, dst) in enumerate(pairs):
            copy = remote(src, dst.at[me], send.at[i, d], recv.at[i, d], counterpart(d))
            copy.start()
            started.append(copy)
    down_load = pltpu.make_async_copy(down_hbm, down_buf, down_sem)
    down_load.start()

    def forward(d):
        source = at(chips - d) * 2 + core
        for i, (src, dst) in enumerate(pairs):
            remote(src, dst.at[source], send.at[i, d], recv.at[i, d], partner).wait_recv()
            copy = remote(dst.at[source], dst.at[source], fsend.at[i, d], frecv.at[i, d], partner)
            copy.start()
            started.append(copy)

    def arrive(d):
        source = at(chips - d) * 2 + 1 - core
        for i, (src, dst) in enumerate(pairs):
            remote(src, dst.at[source], fsend.at[i, d], frecv.at[i, d], partner).wait_recv()

    lane = lax.broadcasted_iota(jnp.int32, (group, 128), 1) // slots

    def up_step(d, base):
        for b in range(2):
            for k in range(side):
                half = k // per_tile
                here = all_aux[base + b, 0, :, half * 128:(half + 1) * 128].astype(jnp.int32) - first
                fits = (here >= 0) & (here < experts) & (lane == k % per_tile)
                where = pl.ds(b * block + k, group, stride=side)
                hi_ref[where, :] = jnp.where(fits, here // 128, -1)
                lo_ref[where, :] = here & 127
        acc_ref[...] = jnp.zeros_like(acc_ref)
        if d == 0:
            for load in up_loads:
                load.wait()

        def chunk(c, carry):
            product = lax.dot_general(
                all_tok[pl.ds(base, 2)].reshape(2 * block, width), up_buf[c], (((1,), (1,)), ((), ())),
                preferred_element_type=jnp.float32,
            )
            acc = acc_ref[...]
            hi = hi_ref[...]
            lo = lo_ref[...]
            for i in range(chunk_rows // 128):
                picked = jnp.take_along_axis(
                    product[:, i * 128:(i + 1) * 128], lo, axis=1, mode="promise_in_bounds"
                )
                acc = jnp.where(hi == c * (chunk_rows // 128) + i, picked, acc)
            acc_ref[...] = acc
            return carry

        lax.fori_loop(0, chunks, chunk, 0, unroll=8)
        for b in range(2):
            for half in range(side // per_tile):
                total = None
                for k in range(half * per_tile, (half + 1) * per_tile):
                    piece = acc_ref[pl.ds(b * block + k, group, stride=side), :]
                    total = piece if total is None else total + piece
                pbuf[d, b, :, half * 128:(half + 1) * 128] = total
        copies = []
        for t in range(1, n_tp):
            copy = remote(pbuf.at[d], pgot.at[d, t], psend.at[d, t], precv.at[d, t], tp_peer(t))
            copy.start()
            copies.append(copy)
        started.extend(copies)
        return copies

    def row_keys(count):
        keys = lax.broadcasted_iota(jnp.int32, (count, lanes), 0).astype(jnp.float32)
        return keys.astype(jnp.bfloat16).reshape(count // 16, 16, lanes)

    row_key = row_keys(tiles * side)
    low_key = row_keys(128)
    turn = lax.broadcasted_iota(jnp.int32, (16, lanes), 1) // slots
    zero = jnp.zeros((1, 16, lanes), jnp.bfloat16)
    one = jnp.ones((1, 16, lanes), jnp.bfloat16)

    def narrow(x):
        return x.astype(jnp.float32).astype(jnp.bfloat16)[None]

    def down_step(d, base, copies):
        total = pbuf[d]
        for t, copy in enumerate(copies):
            copy.wait_recv()
            total += pgot[d, t + 1]
        gate = all_aux[pl.ds(base, 2), 1]
        wt_ref[...] = (gate * jax.nn.gelu(total)).astype(jnp.bfloat16).astype(jnp.float32)

        def spread(b, j):
            here = jnp.broadcast_to(all_aux[base + b, 0, pl.ds(j, 1), :], (16, lanes)).astype(jnp.int32) - first
            weight = jnp.broadcast_to(wt_ref[b, pl.ds(j, 1), :], (16, lanes)).astype(jnp.bfloat16)[None]
            fits = (here >= 0) & (here < experts)
            key = narrow(jnp.where(fits, (here // 128) * side + turn, -1))
            left = jnp.where(row_key == key, weight, zero).reshape(tiles * side, lanes)
            right = jnp.where(low_key == narrow(here & 127), one, zero).reshape(128, lanes)
            wide = lax.dot_general(left, right, (((1,), (1,)), ((), ())), preferred_element_type=jnp.float32)
            return wide.reshape(tiles, side, 128)

        def build(x, carry):
            b = x // (group // 2)
            j = lax.rem(x, group // 2) * 2
            both = jnp.concatenate([spread(b, j), spread(b, j + 1)], axis=1).astype(jnp.bfloat16)
            for h in range(tiles):
                w_ref[pl.ds(pl.multiple_of(x * 2 * side, 2 * side), 2 * side), h * 128:(h + 1) * 128] = both[h]
            return carry

        lax.fori_loop(0, group, build, 0, unroll=8)
        if d == 1:
            down_load.wait()
        sums = jnp.dot(w_ref[...], down_buf[...], preferred_element_type=jnp.float32)
        low, high = sums[:block], sums[block:]
        own[d] = jnp.where(core == 0, low, high)
        xbuf[d] = jnp.where(core == 0, high, low).astype(jnp.bfloat16)
        copy = remote(xbuf.at[d], ybuf.at[d], xsend.at[d], xrecv.at[d], partner)
        copy.start()
        started.append(copy)
        return copy

    returned = []

    def finish(d, copy):
        copy.wait_recv()
        if d == 0:
            return
        sbuf[d] = (own[d] + ybuf[d].astype(jnp.float32)).astype(jnp.bfloat16)
        copy = remote(sbuf.at[d], rbuf.at[d], rsend.at[d], rrecv.at[d], counterpart(chips - d))
        copy.start()
        returned.append(copy)

    def base_of(d):
        return at(chips - d) * 2 if d else chip * 2

    for copy in local:
        copy.wait()
    sending = []
    exchanged = []

    def down_and_finish(d):
        exchanged.append((d, down_step(d, base_of(d), sending[d])))
        if len(exchanged) > 1:
            finish(*exchanged[-2])

    for d in range(chips):
        arrive(d)
        sending.append(up_step(d, base_of(d)))
        if d + 1 < chips:
            forward(d + 1)
        if d > 1:
            down_and_finish(d - 1)
    down_and_finish(chips - 1)
    down_and_finish(0)
    finish(*exchanged[-1])
    total = own[0] + ybuf[0].astype(jnp.float32)
    for d, copy in enumerate(returned):
        copy.wait_recv()
        total += rbuf[d + 1].astype(jnp.float32)
    out_ref[...] = total.astype(jnp.bfloat16)
    for copy in started + returned:
        copy.wait_send()


def on_device(tokens, owner_shard, local_row, gate_weights, up_table, down_table):
    n_ep, n_tp = lax.axis_size("ep"), lax.axis_size("tp")
    count, width = tokens.shape
    slots = gate_weights.shape[1]
    experts = up_table.shape[0]
    side = 8
    group, lanes = count // side, side * slots
    chips = n_ep // 2
    ids = owner_shard[:, 0] * experts + local_row[:, 0]
    aux = jnp.stack([ids.astype(jnp.float32).reshape(group, lanes), gate_weights.reshape(group, lanes)])
    dma = pltpu.SemaphoreType.DMA
    chunks = experts // 512
    wide = (chips, count, width)
    anywhere = pl.BlockSpec(memory_space=pl.ANY)
    return pl.pallas_call(
        functools.partial(fused_kernel, n_ep, n_tp, slots),
        out_shape=jax.ShapeDtypeStruct((count, width), jnp.bfloat16),
        in_specs=[vmem(), vmem(), anywhere, anywhere],
        out_specs=vmem(),
        scratch_shapes=[
            pltpu.VMEM((n_ep, count, width), jnp.bfloat16),
            pltpu.VMEM((n_ep, 2, group, lanes), jnp.float32),
            pltpu.VMEM((chunks, experts // chunks, width), jnp.bfloat16),
            pltpu.VMEM((experts, width), jnp.bfloat16),
            pltpu.VMEM((2 * count, 128), jnp.int32),
            pltpu.VMEM((2 * count, 128), jnp.int32),
            pltpu.VMEM((2 * count, 128), jnp.float32),
            pltpu.VMEM((chips, 2, group, lanes), jnp.float32),
            pltpu.VMEM((chips, n_tp, 2, group, lanes), jnp.float32),
            pltpu.VMEM((2, group, lanes), jnp.float32),
            pltpu.VMEM((2 * count, experts), jnp.bfloat16),
            pltpu.VMEM(wide, jnp.float32),
            pltpu.VMEM(wide, jnp.bfloat16),
            pltpu.VMEM(wide, jnp.bfloat16),
            pltpu.VMEM(wide, jnp.bfloat16),
            pltpu.VMEM(wide, jnp.bfloat16),
            dma((2,)), dma((2, chips)), dma((2, chips)), dma((2, chips)), dma((2, chips)),
            dma((chunks,)), dma, dma((chips, n_tp)), dma((chips, n_tp)),
            dma((chips,)), dma((chips,)), dma((chips,)), dma((chips,)),
        ],
        compiler_params=params(0),
        name="retrieve",
    )(tokens, aux, up_table, down_table)


def solution(mesh):
    return jax.shard_map(
        on_device,
        mesh=mesh,
        in_specs=(
            P("ep", "tp"),
            P("ep", None),
            P("ep", None),
            P("ep", None),
            P("ep", "tp"),
            P("ep", "tp"),
        ),
        out_specs=P("ep", "tp"),
        check_vma=False,
    )
```

profile of v0, /device:TPU:0, one launch (start us, length us, event | category | flops | bytes accessed | tf_op | source)
XLA Modules:
  0.0 53.8 jit_solution(10119988383822812236)
XLA Ops:
  0.0 0.8 %convert_reduce_fusion = f32[4096]{0:T(1024)S(1)} fusion(s32[4096,1]{0,1:T(1,128)} %param.8, s32[4096,1]{0,1:T(1,128)} %param.7), kind=kLoop, calls=%fused_computation.1 | loop fusion | flops 12288 | bytes 49152 | tf_op jit(solution)/shard_map/convert_element_type | solution.py:256
  0.8 0.8 %copy.8 = f32[128,32]{1,0:T(8,128)S(1)} copy(f32[128,32]{0,1:T(8,128)} %param.9) | data formatting | bytes 32768 | tf_op args[3]
  1.6 0.1 stack_reshape.4
  1.7 0.6 %pad_maximum_fusion.aux_ref = f32[2,16,256]{2,1,0:T(8,128)} fusion(f32[1,16,256]{2,1,0:T(8,128)S(1)} %stack_reshape.4, f32[1,16,256]{2,1,0:T(8,128)S(1)} %convert_element_type.14), kind=kLoop, calls=%fused_computation | loop fusion | flops 8192 | bytes 65536 | tf_op jit(solution)/shard_map/stack | solution.py:256
  2.3 49.9 %retrieve.1 = bf16[128,512]{1,0:T(8,128)(2,1)} custom-call(bf16[128,512]{1,0:T(8,128)(2,1)} %tok_ref.1, f32[2,16,256]{2,1,0:T(8,128)} %pad_maximum_fusion.aux_ref, bf16[4096,512]{1,0:T(8,128)(2,1)} %up_hbm.1, bf16[4096,512]{1,0:T(8,128)(2,1)} %down_hbm.1), custom_call_target="tpu_custom_call" | custom-call | tf_op jit(solution)/shard_map/retrieve/pallas_call | solution.py:261
  52.3 1.6 %copy.10 = bf16[128,512]{1,0:T(8,128)(2,1)} copy(bf16[128,512]{1,0:T(8,128)(2,1)} %retrieve.1) | data formatting | bytes 262144
  (1 shorter events, 0.0 us)
where the time goes:
time: 54.3 us; the launch traced here: 53.8 us
  Pallas kernels  49.9 us (92%)
  local copies, waits for them, and re-layouts  2.47 us (5%)
  other arithmetic  1.41 us (3%)
    pallas_call x1, Pallas kernels, on_device(): pl.pallas_call(functools.partial(fused_kernel, n_ep, n_tp, slots), out_sh...  49.9 us
    unnamed x2, local copies, waits for them, and re-layouts  2.38 us

commit v1 on v0

--- a/solution.py
+++ b/solution.py
@@ -8,7 +8,7 @@
 from jax.sharding import PartitionSpec as P
 
 MESH = pl.DeviceIdType.MESH
-VMEM_BYTES = 60 * 1024 * 1024
+VMEM_BYTES = 52 * 1024 * 1024
 
 
 def params(number):
@@ -38,7 +38,7 @@
 def fused_kernel(n_ep, n_tp, slots, tok_ref, aux_ref, up_hbm, down_hbm, out_ref,
                  all_tok, all_aux, up_buf, down_buf, hi_ref, lo_ref, acc_ref, pbuf, pgot, wt_ref, w_ref,
                  own, xbuf, ybuf, sbuf, rbuf,
-                 local_sem, send, recv, fsend, frecv, up_sem, down_sem, psend, precv,
+                 local_sem, send, recv, fsend, frecv, asend, arecv, up_sem, down_sem, psend, precv,
                  xsend, xrecv, rsend, rrecv):
     chips = n_ep // 2
     me = lax.axis_index("ep")
@@ -56,7 +56,12 @@
     per_tile = 128 // slots
 
     def at(step):
-        return lax.rem(chip + step, chips)
+        place = chip
+        for power in range(chips.bit_length() - 1):
+            bit = 1 << power
+            if step & bit:
+                place = place + bit - 2 * bit * lax.rem(chip // bit, 2)
+        return place
 
     def counterpart(step):
         return {"ep": at(step) * 2 + core}
@@ -81,24 +86,65 @@
         copy = remote(src, dst.at[me], fsend.at[i, 0], frecv.at[i, 0], partner)
         copy.start()
         started.append(copy)
-    for d in range(1, chips):
-        for i, (src, dst) in enumerate(pairs):
-            copy = remote(src, dst.at[me], send.at[i, d], recv.at[i, d], counterpart(d))
-            copy.start()
-            started.append(copy)
+
+    halves = group // 8
+    parts = 2 * halves
+
+    def piece(ref, number):
+        rows = pl.ds(pl.multiple_of(lax.rem(number, halves) * 8, 8), 8)
+        return ref.at[number // halves, rows]
+
+    def guarded(number, action):
+        if n_tp <= parts:
+            action()
+        else:
+            pl.when(number < parts)(action)
+
+    def aux_across(d):
+        return remote(piece(aux_ref, part), piece(all_aux.at[me], part), send.at[0, d], recv.at[0, d], counterpart(d))
+
+    def aux_around(d, t):
+        slot = piece(all_aux.at[at(d) * 2 + core], part)
+        return remote(slot, slot, asend.at[d, t], arecv.at[d, t], tp_peer(t))
+
+    order = list(range(2, chips))[:1] + [1] + list(range(3, chips))
+    for d in order:
+        guarded(part, lambda: aux_across(d).start())
+    for d in order:
+        copy = remote(tok_ref, all_tok.at[me], send.at[1, d], recv.at[1, d], counterpart(d))
+        copy.start()
+        started.append(copy)
     down_load = pltpu.make_async_copy(down_hbm, down_buf, down_sem)
     down_load.start()
 
+    def spread_aux(d):
+        def pass_on():
+            aux_across(d).wait_recv()
+            for t in range(1, n_tp):
+                aux_around(d, t).start()
+
+        guarded(part, pass_on)
+
     def forward(d):
-        source = at(chips - d) * 2 + core
+        source = at(d) * 2 + core
+        for t in range(1, n_tp):
+            guarded(lax.rem(part + n_tp - t, n_tp), lambda: aux_around(d, t).wait_recv())
+        remote(tok_ref, all_tok.at[source], send.at[1, d], recv.at[1, d], partner).wait_recv()
         for i, (src, dst) in enumerate(pairs):
-            remote(src, dst.at[source], send.at[i, d], recv.at[i, d], partner).wait_recv()
             copy = remote(dst.at[source], dst.at[source], fsend.at[i, d], frecv.at[i, d], partner)
             copy.start()
             started.append(copy)
 
+    def settle_aux(d):
+        def settle():
+            aux_across(d).wait_send()
+            for t in range(1, n_tp):
+                aux_around(d, t).wait_send()
+
+        guarded(part, settle)
+
     def arrive(d):
-        source = at(chips - d) * 2 + 1 - core
+        source = at(d) * 2 + 1 - core
         for i, (src, dst) in enumerate(pairs):
             remote(src, dst.at[source], fsend.at[i, d], frecv.at[i, d], partner).wait_recv()
 
@@ -123,15 +169,18 @@
                 all_tok[pl.ds(base, 2)].reshape(2 * block, width), up_buf[c], (((1,), (1,)), ((), ())),
                 preferred_element_type=jnp.float32,
             )
-            acc = acc_ref[...]
-            hi = hi_ref[...]
-            lo = lo_ref[...]
-            for i in range(chunk_rows // 128):
-                picked = jnp.take_along_axis(
-                    product[:, i * 128:(i + 1) * 128], lo, axis=1, mode="promise_in_bounds"
-                )
-                acc = jnp.where(hi == c * (chunk_rows // 128) + i, picked, acc)
-            acc_ref[...] = acc
+            here = chunk_rows // 128
+            for r in range(0, 2 * block, 8):
+                rows = slice(r, r + 8)
+                acc = acc_ref[rows, :]
+                hi = hi_ref[rows, :] - c * here
+                lo = lo_ref[rows, :]
+                for i in range(here):
+                    picked = jnp.take_along_axis(
+                        product[rows, i * 128:(i + 1) * 128], lo, axis=1, mode="promise_in_bounds"
+                    )
+                    acc = jnp.where(hi == i, picked, acc)
+                acc_ref[rows, :] = acc
             return carry
 
         lax.fori_loop(0, chunks, chunk, 0, unroll=8)
@@ -163,6 +212,10 @@
     def narrow(x):
         return x.astype(jnp.float32).astype(jnp.bfloat16)[None]
 
+    pending = []
+    returned = []
+    places = []
+
     def down_step(d, base, copies):
         total = pbuf[d]
         for t, copy in enumerate(copies):
@@ -190,7 +243,9 @@
             return carry
 
         lax.fori_loop(0, group, build, 0, unroll=8)
-        if d == 1:
+        if pending:
+            finish(*pending.pop())
+        if d == 0:
             down_load.wait()
         sums = jnp.dot(w_ref[...], down_buf[...], preferred_element_type=jnp.float32)
         low, high = sums[:block], sums[block:]
@@ -201,45 +256,54 @@
         started.append(copy)
         return copy
 
-    returned = []
-
     def finish(d, copy):
         copy.wait_recv()
         if d == 0:
             return
         sbuf[d] = (own[d] + ybuf[d].astype(jnp.float32)).astype(jnp.bfloat16)
-        copy = remote(sbuf.at[d], rbuf.at[d], rsend.at[d], rrecv.at[d], counterpart(chips - d))
+        copy = remote(sbuf.at[d], rbuf.at[d], rsend.at[d], rrecv.at[d], counterpart(d))
         copy.start()
         returned.append(copy)
+        places.append(d)
 
     def base_of(d):
-        return at(chips - d) * 2 if d else chip * 2
+        return at(d) * 2 if d else chip * 2
 
     for copy in local:
         copy.wait()
-    sending = []
-    exchanged = []
-
-    def down_and_finish(d):
-        exchanged.append((d, down_step(d, base_of(d), sending[d])))
-        if len(exchanged) > 1:
-            finish(*exchanged[-2])
-
-    for d in range(chips):
+    sending = {}
+
+    def up(d):
         arrive(d)
-        sending.append(up_step(d, base_of(d)))
-        if d + 1 < chips:
-            forward(d + 1)
-        if d > 1:
-            down_and_finish(d - 1)
-    down_and_finish(chips - 1)
-    down_and_finish(0)
-    finish(*exchanged[-1])
+        sending[d] = up_step(d, base_of(d))
+
+    def down(d):
+        pending.append((d, down_step(d, base_of(d), sending[d])))
+
+    up(0)
+    for d in order:
+        spread_aux(d)
+    down(0)
+    early, late = order[:2], order[2:]
+    for d in early:
+        forward(d)
+        up(d)
+    for d in late:
+        forward(d)
+    down(early[0])
+    for d in late:
+        up(d)
+    down(early[1])
+    for d in late:
+        down(d)
+    finish(*pending.pop())
     total = own[0] + ybuf[0].astype(jnp.float32)
     for d, copy in enumerate(returned):
         copy.wait_recv()
-        total += rbuf[d + 1].astype(jnp.float32)
+        total += rbuf[places[d]].astype(jnp.float32)
     out_ref[...] = total.astype(jnp.bfloat16)
+    for d in range(1, chips):
+        settle_aux(d)
     for copy in started + returned:
         copy.wait_send()
 
@@ -280,7 +344,7 @@
             pltpu.VMEM(wide, jnp.bfloat16),
             pltpu.VMEM(wide, jnp.bfloat16),
             pltpu.VMEM(wide, jnp.bfloat16),
-            dma((2,)), dma((2, chips)), dma((2, chips)), dma((2, chips)), dma((2, chips)),
+            dma((2,)), dma((2, chips)), dma((2, chips)), dma((2, chips)), dma((2, chips)), dma((chips, n_tp)), dma((chips, n_tp)),
             dma((chunks,)), dma, dma((chips, n_tp)), dma((chips, n_tp)),
             dma((chips,)), dma((chips,)), dma((chips,)), dma((chips,)),
         ],

time: 54.3 us -> 46.9 us (0.86)
  Pallas kernels: 49.9 us -> 43.2 us
  other arithmetic: 1.41 us -> 0.79 us
    pallas_call x1, Pallas kernels: 49.9 us -> 43.2 us  [on_device(): pl.pallas_call(functools.partial(fused_kernel, n_ep, n_tp, slots), out_sh...]
    another operation x1, other arithmetic: 0.62 us -> 0.01 us  [on_device(): jnp.stack([ids.astype(jnp.float32).reshape(group, lanes), gate_weights.re...]
    unnamed x2 -> x4, local copies, waits for them, and re-layouts: 2.38 us -> 2.37 us
where the time goes in v1:
time: 46.9 us; the launch traced here: 46.5 us
  Pallas kernels  43.2 us (92%)
  local copies, waits for them, and re-layouts  2.46 us (5%)
  other arithmetic  0.79 us (2%)
    pallas_call x1, Pallas kernels, on_device(): pl.pallas_call(functools.partial(fused_kernel, n_ep, n_tp, slots), out_sh...  43.2 us
    unnamed x4, local copies, waits for them, and re-layouts  2.37 us

profile of v1, /device:TPU:0, one launch (start us, length us, event | category | flops | bytes accessed | tf_op | source)
XLA Modules:
  0.0 46.5 jit_solution(13023599558476157013)
XLA Ops:
  0.0 0.8 %convert_reduce_fusion = f32[4096]{0:T(1024)S(1)} fusion(s32[4096,1]{0,1:T(1,128)} %param.8, s32[4096,1]{0,1:T(1,128)} %param.7), kind=kLoop, calls=%fused_computation.1 | loop fusion | flops 12288 | bytes 49152 | tf_op jit(solution)/shard_map/convert_element_type | solution.py:320
  0.8 0.8 %copy.8 = f32[128,32]{1,0:T(8,128)S(1)} copy(f32[128,32]{0,1:T(8,128)} %param.9) | data formatting | bytes 32768 | tf_op args[3]
  1.6 0.1 stack_reshape.4
  1.7 0.0 copy-start
  1.7 0.9 %copy-done = bf16[128,512]{1,0:T(8,128)(2,1)S(1)} copy-done((bf16[128,512]{1,0:T(8,128)(2,1)S(1)}, bf16[128,512]{1,0:T(8,128)(2,1)}, u32[]{:S(2)}) %copy-start) | copy-done | bytes 131096
  2.6 43.2 %retrieve.1 = bf16[128,512]{1,0:T(8,128)(2,1)S(1)} custom-call(bf16[128,512]{1,0:T(8,128)(2,1)S(1)} %copy-done, f32[2,16,256]{2,1,0:T(8,128)S(1)} %pad_maximum_fusion.aux_ref, bf16[4096,512]{1,0:T(8,128)(2,1)} %up_hbm.1, bf16[4096,512]{1,0:T(8,128)(2,1)} %down_hbm.1), custom_call_target="tpu_custom_call" | custom-call | tf_op jit(solution)/shard_map/retrieve/pallas_call | solution.py:325
  45.8 0.7 %copy.10 = bf16[128,512]{1,0:T(8,128)(2,1)} copy(bf16[128,512]{1,0:T(8,128)(2,1)S(1)} %retrieve.1) | data formatting | bytes 262144
  (2 shorter events, 0.0 us)
Async XLA Ops:
  1.7 0.9 %copy-start = (bf16[128,512]{1,0:T(8,128)(2,1)S(1)}, bf16[128,512]{1,0:T(8,128)(2,1)}, u32[]{:S(2)}) copy-start(bf16[128,512]{1,0:T(8,128)(2,1)} %tok_ref.1) | copy-start | bytes 393220

commit v2 on v1

--- a/solution.py
+++ b/solution.py
@@ -35,8 +35,8 @@
     )
 
 
-def fused_kernel(n_ep, n_tp, slots, tok_ref, aux_ref, up_hbm, down_hbm, out_ref,
-                 all_tok, all_aux, up_buf, down_buf, hi_ref, lo_ref, acc_ref, pbuf, pgot, wt_ref, w_ref,
+def fused_kernel(n_ep, n_tp, slots, tok_ref, ids_ref, gate_ref, up_hbm, down_hbm, out_ref,
+                 aux_ref, turned_ref, all_tok, all_aux, up_buf, down_buf, hi_ref, lo_ref, acc_ref, pbuf, pgot, wt_ref, w_ref,
                  own, xbuf, ybuf, sbuf, rbuf,
                  local_sem, send, recv, fsend, frecv, asend, arecv, up_sem, down_sem, psend, precv,
                  xsend, xrecv, rsend, rrecv):
@@ -74,6 +74,16 @@
         load = pltpu.make_async_copy(up_hbm.at[pl.ds(c * chunk_rows, chunk_rows)], up_buf.at[c], up_sem.at[c])
         load.start()
         up_loads.append(load)
+    turned_ref[...] = jnp.concatenate([gate_ref[...]] * per_tile, axis=0).T
+    place = lax.broadcasted_iota(jnp.int32, (group, 128), 1) // slots
+    for half in range(side // per_tile):
+        columns = slice(half * 128, (half + 1) * 128)
+        aux_ref[0, :, columns] = ids_ref[pl.ds(half, group, stride=lanes // 128), :]
+        gates = turned_ref[pl.ds(half * per_tile, group, stride=side), :]
+        for k in range(1, per_tile):
+            rows = pl.ds(half * per_tile + k, group, stride=side)
+            gates = jnp.where(place == k, turned_ref[rows, :], gates)
+        aux_ref[1, :, columns] = gates
     greet([partner] + [counterpart(d) for d in range(1, chips)] + [tp_peer(d) for d in range(1, n_tp)])
 
     pairs = ((aux_ref, all_aux), (tok_ref, all_tok))
@@ -107,13 +117,18 @@
         slot = piece(all_aux.at[at(d) * 2 + core], part)
         return remote(slot, slot, asend.at[d, t], arecv.at[d, t], tp_peer(t))
 
-    order = list(range(2, chips))[:1] + [1] + list(range(3, chips))
-    for d in order:
+    def aux_whole():
+        return remote(aux_ref, all_aux.at[me], send.at[0, 1], recv.at[0, 1], counterpart(1))
+
+    aux_whole().start()
+    for d in range(2, chips):
         guarded(part, lambda: aux_across(d).start())
-    for d in order:
+    def send_tokens(d):
         copy = remote(tok_ref, all_tok.at[me], send.at[1, d], recv.at[1, d], counterpart(d))
         copy.start()
         started.append(copy)
+
+    send_tokens(1)
     down_load = pltpu.make_async_copy(down_hbm, down_buf, down_sem)
     down_load.start()
 
@@ -127,7 +142,9 @@
 
     def forward(d):
         source = at(d) * 2 + core
-        for t in range(1, n_tp):
+        if d == 1:
+            aux_whole().wait_recv()
+        for t in range(1, n_tp if d > 1 else 1):
             guarded(lax.rem(part + n_tp - t, n_tp), lambda: aux_around(d, t).wait_recv())
         remote(tok_ref, all_tok.at[source], send.at[1, d], recv.at[1, d], partner).wait_recv()
         for i, (src, dst) in enumerate(pairs):
@@ -192,6 +209,8 @@
                     total = piece if total is None else total + piece
                 pbuf[d, b, :, half * 128:(half + 1) * 128] = total
         copies = []
+        if pending:
+            finish(*pending.pop())
         for t in range(1, n_tp):
             copy = remote(pbuf.at[d], pgot.at[d, t], psend.at[d, t], precv.at[d, t], tp_peer(t))
             copy.start()
@@ -274,35 +293,42 @@
     sending = {}
 
     def up(d):
-        arrive(d)
+        if d:
+            arrive(d)
         sending[d] = up_step(d, base_of(d))
 
     def down(d):
         pending.append((d, down_step(d, base_of(d), sending[d])))
 
+    arrive(0)
+    last = chips - 1
+    send_tokens(2)
     up(0)
-    for d in order:
+    for d in range(3, chips):
+        send_tokens(d)
+    forward(1)
+    for d in range(2, chips):
         spread_aux(d)
+    up(1)
+    forward(2)
+    up(2)
+    forward(3)
     down(0)
-    early, late = order[:2], order[2:]
-    for d in early:
-        forward(d)
-        up(d)
-    for d in late:
-        forward(d)
-    down(early[0])
-    for d in late:
-        up(d)
-    down(early[1])
-    for d in late:
+    for d in range(2, last):
         down(d)
+        up(d + 1)
+        if d + 2 < chips:
+            forward(d + 2)
+    down(1)
+    down(last)
     finish(*pending.pop())
     total = own[0] + ybuf[0].astype(jnp.float32)
     for d, copy in enumerate(returned):
         copy.wait_recv()
         total += rbuf[places[d]].astype(jnp.float32)
     out_ref[...] = total.astype(jnp.bfloat16)
-    for d in range(1, chips):
+    aux_whole().wait_send()
+    for d in range(2, chips):
         settle_aux(d)
     for copy in started + returned:
         copy.wait_send()
@@ -316,8 +342,8 @@
     side = 8
     group, lanes = count // side, side * slots
     chips = n_ep // 2
-    ids = owner_shard[:, 0] * experts + local_row[:, 0]
-    aux = jnp.stack([ids.astype(jnp.float32).reshape(group, lanes), gate_weights.reshape(group, lanes)])
+    dense = (count * slots // 128, 128)
+    ids = (owner_shard[:, 0] * experts + local_row[:, 0]).astype(jnp.float32)
     dma = pltpu.SemaphoreType.DMA
     chunks = experts // 512
     wide = (chips, count, width)
@@ -325,9 +351,11 @@
     return pl.pallas_call(
         functools.partial(fused_kernel, n_ep, n_tp, slots),
         out_shape=jax.ShapeDtypeStruct((count, width), jnp.bfloat16),
-        in_specs=[vmem(), vmem(), anywhere, anywhere],
+        in_specs=[vmem(), vmem(), vmem(), anywhere, anywhere],
         out_specs=vmem(),
         scratch_shapes=[
+            pltpu.VMEM((2, group, lanes), jnp.float32),
+            pltpu.VMEM((count, 128), jnp.float32),
             pltpu.VMEM((n_ep, count, width), jnp.bfloat16),
             pltpu.VMEM((n_ep, 2, group, lanes), jnp.float32),
             pltpu.VMEM((chunks, experts // chunks, width), jnp.bfloat16),
@@ -350,7 +378,7 @@
         ],
         compiler_params=params(0),
         name="retrieve",
-    )(tokens, aux, up_table, down_table)
+    )(tokens, ids.reshape(dense), gate_weights.T, up_table, down_table)
 
 
 def solution(mesh):

time: 46.9 us -> 46.1 us (0.983)
  Pallas kernels: 43.2 us -> 42.6 us
    pallas_call x1, Pallas kernels: 43.2 us -> 42.6 us  [on_device(): pl.pallas_call(functools.partial(fused_kernel, n_ep, n_tp, slots), out_sh...]
    unnamed x4 -> x5, local copies, waits for them, and re-layouts: 2.37 us -> 2.27 us
where the time goes in v2:
time: 46.1 us; the launch traced here: 45.7 us
  Pallas kernels  42.6 us (92%)
  local copies, waits for them, and re-layouts  2.27 us (5%)
  other arithmetic  0.76 us (2%)
    pallas_call x1, Pallas kernels, on_device(): pl.pallas_call(functools.partial(fused_kernel, n_ep, n_tp, slots), out_sh...  42.6 us
    unnamed x5, local copies, waits for them, and re-layouts  2.27 us

profile of v2, /device:TPU:0, one launch (start us, length us, event | category | flops | bytes accessed | tf_op | source)
XLA Modules:
  0.0 45.7 jit_solution(3918663485841792189)
XLA Ops:
  0.0 0.8 %add_convert_fusion = f32[4096,1]{0,1:T(1,128)S(1)} fusion(s32[4096,1]{0,1:T(1,128)} %param.8, s32[4096,1]{0,1:T(1,128)} %param.7), kind=kLoop, calls=%fused_computation | loop fusion | flops 12288 | bytes 49152 | tf_op jit(solution)/shard_map/convert_element_type | solution.py:346
  0.8 0.0 copy-start
  0.8 0.9 %copy-done = bf16[128,512]{1,0:T(8,128)(2,1)S(1)} copy-done((bf16[128,512]{1,0:T(8,128)(2,1)S(1)}, bf16[128,512]{1,0:T(8,128)(2,1)}, u32[]{:S(2)}) %copy-start) | copy-done | bytes 131096
  1.7 0.0 copy-start.1
  1.7 0.7 %copy-done.1 = f32[128,32]{0,1:T(8,128)S(1)} copy-done((f32[128,32]{0,1:T(8,128)S(1)}, f32[128,32]{0,1:T(8,128)}, u32[]{:S(2)}) %copy-start.1) | copy-done | bytes 16408
  2.4 42.6 %retrieve.1 = bf16[128,512]{1,0:T(8,128)(2,1)S(1)} custom-call(bf16[128,512]{1,0:T(8,128)(2,1)S(1)} %copy-done, f32[32,128]{1,0:T(8,128)S(1)} %bitcast.2, f32[32,128]{1,0:T(8,128)S(1)} %bitcast.3, bf16[4096,512]{1,0:T(8,128)(2,1)} %up_hbm.1, bf16[4096,512]{1,0:T(8,128)(2,1)} %down_hbm.1), custom_call_target="tpu_custom_call" | custom-call | tf_op jit(solution)/shard_map/retrieve/pallas_call | solution.py:351
  45.0 0.7 %copy.8 = bf16[128,512]{1,0:T(8,128)(2,1)} copy(bf16[128,512]{1,0:T(8,128)(2,1)S(1)} %retrieve.1) | data formatting | bytes 262144
Async XLA Ops:
  0.8 0.9 %copy-start = (bf16[128,512]{1,0:T(8,128)(2,1)S(1)}, bf16[128,512]{1,0:T(8,128)(2,1)}, u32[]{:S(2)}) copy-start(bf16[128,512]{1,0:T(8,128)(2,1)} %tok_ref.1) | copy-start | bytes 393220
  1.7 0.7 %copy-start.1 = (f32[128,32]{0,1:T(8,128)S(1)}, f32[128,32]{0,1:T(8,128)}, u32[]{:S(2)}) copy-start(f32[128,32]{0,1:T(8,128)} %param.9) | copy-start | bytes 49156
